TPU v7x, 32 devices: a whole 2x2x4 slice. The times are simulated.
32 devices in a mesh: grp: 2 (over y), sp: 4 (over z), tp: 4 (over x, core).
Axes of the slice: x: 2, y: 2, z: 4, core: 2. Of those that a mesh axis runs over, the one named last changes fastest.
Arguments:
- stream: bfloat16 [2048, 4096], P(('grp', 'sp'), 'tp'), parts along dimension 0, may hold values from -6 to 6
- gain_pre: float32 [3, 4096], replicated, may hold values from 0.1 to 1.9
- w_in: bfloat16 [3, 4096, 1024], P(None, 'sp', 'tp'), may hold values from -0.09375 to 0.09375
- w_pool: bfloat16 [3, 4, 256, 256], P(None, 'tp'), may hold values from -0.375 to 0.375
- pool_scale: float32 [3, 1024], P(None, 'tp'), may hold values from 0.1 to 1.9
- w_out: bfloat16 [3, 1024, 4096], P(None, 'tp', 'sp'), may hold values from -0.5 to 0.5
- gain_post: float32 [3, 4096], replicated, may hold values from 0.1 to 1.9
Outputs:
- result: bfloat16 [2048, 4096], P(('grp', 'sp'), 'tp'), parts along dimension 0
There are 2 independent parts, one for each index of `grp`. A program takes and returns all parts, laid end to end along the dimension named above; an argument that names none is the same for every part. Nothing has to cross between parts.
All inputs are finite; a program needn't handle non-finite values.
Results may differ from a plain program's by a relative error of at most 0.02.
Values may be sent and summed in bfloat16 or wider, within the bound.
A program may use at most 64 MiB of HBM per device.

v0:
```python
import jax
import jax.numpy as jnp
from jax import lax
from jax.sharding import PartitionSpec as P

LAYERS = 3
WINDOWS = (2, 4, 8, 16)
EPS = 1e-06


def from_behind(block, axis, distance):
    devices = range(lax.axis_size(axis))
    route = [(i - distance, i) for i in devices if i - distance in devices]
    return lax.ppermute(block, axis, route)


def rms_scale(values, gain):
    inverse = lax.rsqrt(jnp.mean(values * values, axis=-1, keepdims=True) + EPS)
    return values * inverse * gain[None, :]


def per_device(stream, gain_pre, w_in, w_pool, pool_scale, w_out, gain_post):
    tok_rows = stream.shape[0]
    block_width = stream.shape[1]
    width = gain_pre.shape[1]
    group = w_pool.shape[2]
    reach = max(WINDOWS) - 1
    group_index = lax.axis_index("tp")
    window = jnp.where(
        group_index == 0, 2, jnp.where(group_index == 1, 4, jnp.where(group_index == 2, 8, 16))
    )
    positions = lax.axis_index("sp") * tok_rows + lax.iota(jnp.int32, tok_rows)
    count = jnp.minimum(positions + 1, window).astype(jnp.float32)
    gathered_in, gathered_out = (
        lax.all_gather(w_in, "sp", axis=1, tiled=True),
        lax.all_gather(w_out, "sp", axis=2, tiled=True),
    )
    current = stream
    feature_start = group_index * block_width
    for layer in range(LAYERS):
        full_rows = lax.all_gather(current, "tp", axis=1, tiled=True)
        normed = rms_scale(full_rows.astype(jnp.float32), gain_pre[layer]).astype(jnp.bfloat16)
        inner_sum = jnp.dot(normed, gathered_in[layer], preferred_element_type=jnp.float32)
        inner = inner_sum.astype(jnp.bfloat16)
        rim = from_behind(inner[tok_rows - reach :], "sp", 1)
        extended = jnp.concatenate([rim, inner], axis=0).astype(jnp.float32)
        summed = jnp.zeros((tok_rows, group), jnp.float32)
        for offset in range(max(WINDOWS)):
            window_slice = extended[reach - offset : reach - offset + tok_rows]
            summed = summed + jnp.where(offset < window, window_slice, 0.0)
        pooled = summed / count[:, None]
        spread = (pooled - inner.astype(jnp.float32)).astype(jnp.bfloat16)
        mixed = jnp.dot(spread, w_pool[layer, 0], preferred_element_type=jnp.float32)
        mixed = (mixed * pool_scale[layer][None, :]).astype(jnp.bfloat16)
        partial_value = jnp.dot(mixed, gathered_out[layer], preferred_element_type=jnp.float32)
        partial_value = partial_value.astype(jnp.bfloat16)
        branch = lax.psum_scatter(partial_value, "tp", scatter_dimension=1, tiled=True).astype(
            jnp.float32
        )
        squares = lax.psum(jnp.sum(branch * branch, axis=1), "tp")
        inverse = lax.rsqrt(squares / width + EPS)
        gain_block = lax.dynamic_slice_in_dim(gain_post[layer], feature_start, block_width, 0)
        normed_branch = branch * inverse[:, None] * gain_block[None, :]
        current = (current.astype(jnp.float32) + normed_branch).astype(jnp.bfloat16)
    return current


def solution(mesh):
    return jax.shard_map(
        per_device,
        mesh=mesh,
        in_specs=(
            P(("grp", "sp"), "tp"),
            P(),
            P(None, "sp", "tp"),
            P(None, "tp", None, None),
            P(None, "tp"),
            P(None, "tp", "sp"),
            P(),
        ),
        out_specs=P(("grp", "sp"), "tp"),
        check_vma=False,
    )
```

profile of v0, /device:TPU:0, one launch (start us, length us, event | category | flops | bytes accessed | tf_op | source)
XLA Modules:
  0.0 473.9 jit_solution(1717130798795279151)
XLA Ops:
  6.5 0.0 all-gather.6.cloned.1.call-start
  6.5 0.7 all-gather.6.cloned.1.call-update
  7.3 0.0 all-gather.8.cloned.1.call-start
  7.3 0.7 all-gather.8.cloned.1.call-update
  8.0 0.0 all-gather.10.cloned.1.call-start
  8.1 0.7 all-gather.10.cloned.1.call-update
  8.7 0.0 reduce-scatter.4.cloned.1.call-start
  8.8 0.8 fusion.236
  9.6 1.0 fusion.235
  10.6 23.6 %all-gather.6.cloned.1.call-done = bf16[256,4096]{1,0:T(8,128)(2,1)} async-done(((bf16[256,1024]{1,0:T(8,128)(2,1)}), bf16[256,4096]{1,0:T(8,128)(2,1)}) %all-gather.6.cloned.1.call-update) | async-done | bytes 2097168 | tf_op jit(solution)/shard_map/all_gather | solution.py:41
  34.2 2.1 fusion
  36.3 0.0 copy-start.4
  36.3 114.8 %all-gather.8.cloned.1.call-done = bf16[3,4096,256]{2,1,0:T(8,128)(2,1)} async-done(((bf16[3,1024,256]{2,1,0:T(8,128)(2,1)}), bf16[3,4096,256]{2,1,0:T(8,128)(2,1)}) %all-gather.8.cloned.1.call-update) | async-done | bytes 6291472 | tf_op jit(solution)/shard_map/all_gather | solution.py:35
  151.1 3.0 fusion.24
  154.1 1.3 collective-permute-start
  155.5 1.3 collective-permute-done
  156.8 109.5 %all-gather.10.cloned.1.call-done = bf16[3,256,4096]{2,1,0:T(8,128)(2,1)} async-done(((bf16[3,256,1024]{2,1,0:T(8,128)(2,1)}), bf16[3,256,4096]{2,1,0:T(8,128)(2,1)}) %all-gather.10.cloned.1.call-update) | async-done | bytes 6291472 | tf_op jit(solution)/shard_map/all_gather | solution.py:36
  266.3 0.0 copy-done.4
  266.3 0.0 copy-start.3
  266.3 0.0 copy-start.2
  266.3 4.4 convolution_convert_fusion.2
  270.7 0.0 reduce-scatter.4.cloned.1.call-update
  270.7 0.0 all-gather.12.cloned.1.call-start
  270.7 0.0 copy-done.3
  270.8 29.4 %reduce-scatter.4.cloned.1.call-done = bf16[256,1024]{1,0:T(8,128)(2,1)} async-done(((bf16[256,4096]{1,0:T(8,128)(2,1)}), bf16[256,1024]{1,0:T(8,128)(2,1)}) %reduce-scatter.4.cloned.1.call-update) | async-done | bytes 524304 | tf_op jit(solution)/shard_map/reduce_scatter | solution.py:57
  300.2 1.2 fusion.33
  301.4 5.8 %psum.21 = f32[256]{0:T(256)S(1)} all-reduce(f32[256]{0:T(256)S(1)} %fusion.33), channel_id=1, replica_groups=mesh['grp'=2,'sp'=4,'tp'=4] {'tp'}, use_global_device_ids=true, to_apply=%region_3.4 | all-reduce | flops 256 | bytes 2048 | tf_op jit(solution)/shard_map/psum | solution.py:60
  307.2 0.0 copy-done.2
  307.2 2.1 fusion.36
  309.3 0.0 all-gather.12.cloned.1.call-update
  309.3 0.0 reduce-scatter.6.cloned.1.call-start
  309.4 23.3 %all-gather.12.cloned.1.call-done = bf16[256,4096]{1,0:T(8,128)(2,1)} async-done(((bf16[256,1024]{1,0:T(8,128)(2,1)}), bf16[256,4096]{1,0:T(8,128)(2,1)}) %all-gather.12.cloned.1.call-update) | async-done | bytes 2097168 | tf_op jit(solution)/shard_map/all_gather | solution.py:41
  332.7 2.1 fusion.3
  334.7 3.0 fusion.27
  337.8 3.4 collective-permute-start.1
  341.2 1.3 collective-permute-done.1
  342.5 0.0 copy-start.1
  342.5 4.4 convolution_convert_fusion.1
  346.9 0.0 reduce-scatter.6.cloned.1.call-update
  346.9 0.0 all-gather.14.cloned.1.call-start
  347.0 32.0 %reduce-scatter.6.cloned.1.call-done = bf16[256,1024]{1,0:T(8,128)(2,1)} async-done(((bf16[256,4096]{1,0:T(8,128)(2,1)}), bf16[256,1024]{1,0:T(8,128)(2,1)}) %reduce-scatter.6.cloned.1.call-update) | async-done | bytes 524304 | tf_op jit(solution)/shard_map/reduce_scatter | solution.py:57
  379.0 1.2 fusion.37
  380.3 5.8 %psum.22 = f32[256]{0:T(256)S(1)} all-reduce(f32[256]{0:T(256)S(1)} %fusion.37), channel_id=1, replica_groups=mesh['grp'=2,'sp'=4,'tp'=4] {'tp'}, use_global_device_ids=true, to_apply=%region_7.8 | all-reduce | flops 256 | bytes 2048 | tf_op jit(solution)/shard_map/psum | solution.py:60
  386.0 0.0 copy-done.1
  386.0 2.1 fusion.40
  388.1 0.0 all-gather.14.cloned.1.call-update
  388.2 0.0 reduce-scatter.8.cloned.1.call-start
  388.2 23.3 %all-gather.14.cloned.1.call-done = bf16[256,4096]{1,0:T(8,128)(2,1)} async-done(((bf16[256,1024]{1,0:T(8,128)(2,1)}), bf16[256,4096]{1,0:T(8,128)(2,1)}) %all-gather.14.cloned.1.call-update) | async-done | bytes 2097168 | tf_op jit(solution)/shard_map/all_gather | solution.py:41
  411.5 2.1 fusion.6
  413.6 3.0 fusion.30
  416.6 3.4 collective-permute-start.2
  420.0 1.3 collective-permute-done.2
  421.4 0.0 copy-start
  421.4 4.3 convolution_convert_fusion
  425.8 0.0 reduce-scatter.8.cloned.1.call-update
  425.8 32.1 %reduce-scatter.8.cloned.1.call-done = bf16[256,1024]{1,0:T(8,128)(2,1)} async-done(((bf16[256,4096]{1,0:T(8,128)(2,1)}), bf16[256,1024]{1,0:T(8,128)(2,1)}) %reduce-scatter.8.cloned.1.call-update) | async-done | bytes 524304 | tf_op jit(solution)/shard_map/reduce_scatter | solution.py:57
  457.9 1.2 fusion.41
  459.1 5.8 %psum.23 = f32[256]{0:T(256)S(1)} all-reduce(f32[256]{0:T(256)S(1)} %fusion.41), channel_id=1, replica_groups=mesh['grp'=2,'sp'=4,'tp'=4] {'tp'}, use_global_device_ids=true, to_apply=%region_11.12 | all-reduce | flops 256 | bytes 2048 | tf_op jit(solution)/shard_map/psum | solution.py:60
  464.9 0.0 copy-done
  464.9 2.1 fusion.44
  (17 shorter events, 0.2 us)
Async XLA Ops:
  6.5 27.7 %all-gather.6.cloned.1.call-start = ((), (), s32[]{:S(2)}) async-start(), calls=%async_computation.3 | async-start | bytes 2621440 | tf_op jit(solution)/shard_map/all_gather | solution.py:41
  7.3 143.9 %all-gather.8.cloned.1.call-start = ((), (), s32[]{:S(2)}) async-start(), calls=%async_computation.4 | async-start | bytes 7864320 | tf_op jit(solution)/shard_map/all_gather | solution.py:35
  8.0 258.3 %all-gather.10.cloned.1.call-start = ((), (), s32[]{:S(2)}) async-start(), calls=%async_computation.5 | async-start | bytes 7864320 | tf_op jit(solution)/shard_map/all_gather | solution.py:36
  8.7 291.5 %reduce-scatter.4.cloned.1.call-start = ((), (), s32[]{:S(2)}) async-start(), calls=%async_computation.6 | async-start | bytes 2621440 | tf_op jit(solution)/shard_map/reduce_scatter | solution.py:57
  36.3 230.0 %copy-start.4 = (bf16[3,1,256,256]{3,2,1,0:T(8,128)(2,1)S(1)}, bf16[3,1,256,256]{3,2,1,0:T(8,128)(2,1)}, u32[]{:S(2)}) copy-start(bf16[3,1,256,256]{3,2,1,0:T(8,128)(2,1)} %param.10) | copy-start | bytes 1179652
  154.1 2.6 collective-permute-start
  266.3 4.4 copy-start.3
  266.3 40.9 %copy-start.2 = (bf16[256,1024]{1,0:T(8,128)(2,1)S(1)}, bf16[256,1024]{1,0:T(8,128)(2,1)}, u32[]{:S(2)}) copy-start(bf16[256,1024]{1,0:T(8,128)(2,1)} %param.7) | copy-start | bytes 1572868
  270.7 62.0 %all-gather.12.cloned.1.call-start = ((), (), s32[]{:S(2)}) async-start(), calls=%async_computation.7 | async-start | bytes 2621440 | tf_op jit(solution)/shard_map/all_gather | solution.py:41
  309.3 69.7 %reduce-scatter.6.cloned.1.call-start = ((), (), s32[]{:S(2)}) async-start(), calls=%async_computation.8 | async-start | bytes 2621440 | tf_op jit(solution)/shard_map/reduce_scatter | solution.py:57
  337.8 4.7 %collective-permute-start.1 = (bf16[15,256]{1,0:T(8,128)(2,1)S(1)}, bf16[15,256]{1,0:T(8,128)(2,1)S(1)}, u32[]{:S(2)}, u32[]{:S(2)}) collective-permute-start(bf16[15,256]{1,0:T(8,128)(2,1)S(1)} %slice.296), channel_id=1, source_target_pairs={{0,4},{4,8},{8,12},{1,5},{5,9},{9,13},{2,6},{6,10},{10,14},{3,7},{... | collective-permute-start | bytes 23048 | tf_op jit(solution)/shard_map/ppermute | solution.py:14
  342.5 43.5 %copy-start.1 = (bf16[256,1024]{1,0:T(8,128)(2,1)S(1)}, bf16[256,1024]{1,0:T(8,128)(2,1)}, u32[]{:S(2)}) copy-start(bf16[256,1024]{1,0:T(8,128)(2,1)} %fusion.36) | copy-start | bytes 1572868
  346.9 64.6 %all-gather.14.cloned.1.call-start = ((), (), s32[]{:S(2)}) async-start(), calls=%async_computation.9 | async-start | bytes 2621440 | tf_op jit(solution)/shard_map/all_gather | solution.py:41
  388.2 69.8 %reduce-scatter.8.cloned.1.call-start = ((), (), s32[]{:S(2)}) async-start(), calls=%async_computation.10 | async-start | bytes 2621440 | tf_op jit(solution)/shard_map/reduce_scatter | solution.py:57
  416.6 4.7 %collective-permute-start.2 = (bf16[15,256]{1,0:T(8,128)(2,1)S(1)}, bf16[15,256]{1,0:T(8,128)(2,1)S(1)}, u32[]{:S(2)}, u32[]{:S(2)}) collective-permute-start(bf16[15,256]{1,0:T(8,128)(2,1)S(1)} %slice.315), channel_id=1, source_target_pairs={{0,4},{4,8},{8,12},{1,5},{5,9},{9,13},{2,6},{6,10},{10,14},{3,7},{... | collective-permute-start | bytes 23048 | tf_op jit(solution)/shard_map/ppermute | solution.py:14
  421.4 43.5 %copy-start = (bf16[256,1024]{1,0:T(8,128)(2,1)S(1)}, bf16[256,1024]{1,0:T(8,128)(2,1)}, u32[]{:S(2)}) copy-start(bf16[256,1024]{1,0:T(8,128)(2,1)} %fusion.40) | copy-start | bytes 1572868
Sparse Core Ops, SparseCore 0:
  8.9 25.2 all-gather.5
  35.8 115.3 all-gather.7
  152.7 113.5 all-gather.9
  270.8 29.3 reduce-scatter.3
  309.4 23.1 all-gather.11
  347.1 31.9 reduce-scatter.5
  388.3 23.1 all-gather.13
  425.9 31.9 reduce-scatter.7
where the time goes:
time: 475 us; the launch traced here: 474 us
  waiting for transfers between devices  394 us (83%)
  matrix products  22 us (5%)
  blocking collectives  17.3 us (4%)
  other arithmetic  16.3 us (3%)
  between operations  13.7 us (3%)
  starting transfers between devices  8.35 us (2%)
    all_gather x1, waiting for transfers between devices, per_device(): lax.all_gather(w_in, 'sp', axis=1, tiled=True)  115 us
    all_gather x1, waiting for transfers between devices, per_device(): lax.all_gather(w_out, 'sp', axis=2, tiled=True)  109 us
    reduce_scatter x3, waiting for transfers between devices, per_device(): lax.psum_scatter(partial_value, 'tp', scatter_dimension=1, tiled=True)  93.6 us
    all_gather x3, waiting for transfers between devices, per_device(): full_rows = lax.all_gather(current, 'tp', axis=1, tiled=True)  70.2 us
    psum x3, blocking collectives, per_device(): squares = lax.psum(jnp.sum(branch * branch, axis=1), 'tp')  17.3 us
    dot_general x3, matrix products, per_device(): jnp.dot(mixed, gathered_out[layer], preferred_element_type=jnp.float32)  13.1 us
  transfers between devices with their start and end apart: 11, of which 11 were waited for; matrix products, arithmetic and copies ran while one was open for 1% of the time, Pallas kernels for 0%

commit v1 on v0

--- a/solution.py
+++ b/solution.py
@@ -38,7 +38,16 @@
     current = stream
     feature_start = group_index * block_width
     for layer in range(LAYERS):
-        full_rows = lax.all_gather(current, "tp", axis=1, tiled=True)
+        num_devices = lax.axis_size("tp")
+        left_arr = sorted(((w, (w + 1) % num_devices) for w in range(num_devices)))
+        o_now = current
+        by_rank = [o_now]
+        for ix in range(1, num_devices):
+            o_now = lax.ppermute(o_now, axis_name="tp", perm=left_arr)
+            by_rank.insert(0, o_now)
+        s_next = jnp.concatenate(by_rank, axis=1)
+        main = lax.axis_index("tp") + 1
+        full_rows = jnp.roll(s_next, main * current.shape[1], axis=1)
         normed = rms_scale(full_rows.astype(jnp.float32), gain_pre[layer]).astype(jnp.bfloat16)
         inner_sum = jnp.dot(normed, gathered_in[layer], preferred_element_type=jnp.float32)
         inner = inner_sum.astype(jnp.bfloat16)

time: 475 us -> 457 us (0.962)
  waiting for transfers between devices: 394 us -> 374 us
    ppermute x0 -> x9, waiting for transfers between devices: none -> 76 us  [per_device(): o_now = lax.ppermute(o_now, axis_name='tp', perm=left_arr)]
    all_gather x3 -> x0, waiting for transfers between devices: 70.2 us -> none  [per_device(): full_rows = lax.all_gather(current, 'tp', axis=1, tiled=True)]
    all_gather x1, waiting for transfers between devices: 115 us -> 87.9 us  [per_device(): lax.all_gather(w_in, 'sp', axis=1, tiled=True)]
    reduce_sum x3, other arithmetic: 6.25 us -> 11.6 us  [rms_scale(): inverse = lax.rsqrt(jnp.mean(values * values, axis=-1, keepdims=True) + EPS)]
  transfers between devices with their start and end apart: 11 -> 17, of which waited for: 11 -> 17; matrix products, arithmetic and copies ran while one was open for 1% -> 2% of each run, Pallas kernels for 0% -> 0%
where the time goes in v1:
time: 457 us; the launch traced here: 456 us
  waiting for transfers between devices  374 us (82%)
  matrix products  20.2 us (4%)
  other arithmetic  20.1 us (4%)
  blocking collectives  17.3 us (4%)
  between operations  13.4 us (3%)
  starting transfers between devices  9.28 us (2%)
    all_gather x1, waiting for transfers between devices, per_device(): lax.all_gather(w_out, 'sp', axis=2, tiled=True)  110 us
    reduce_scatter x3, waiting for transfers between devices, per_device(): lax.psum_scatter(partial_value, 'tp', scatter_dimension=1, tiled=True)  94.5 us
    all_gather x1, waiting for transfers between devices, per_device(): lax.all_gather(w_in, 'sp', axis=1, tiled=True)  87.9 us
    ppermute x9, waiting for transfers between devices, per_device(): o_now = lax.ppermute(o_now, axis_name='tp', perm=left_arr)  76 us
    psum x3, blocking collectives, per_device(): squares = lax.psum(jnp.sum(branch * branch, axis=1), 'tp')  17.3 us
    dot_general x3, matrix products, per_device(): jnp.dot(mixed, gathered_out[layer], preferred_element_type=jnp.float32)  13 us
    reduce_sum x3, other arithmetic, rms_scale(): inverse = lax.rsqrt(jnp.mean(values * values, axis=-1, keepdims=True) + EPS)  11.6 us
  transfers between devices with their start and end apart: 17, of which 17 were waited for; matrix products, arithmetic and copies ran while one was open for 2% of the time, Pallas kernels for 0%

profile of v1, /device:TPU:0, one launch (start us, length us, event | category | flops | bytes accessed | tf_op | source)
XLA Modules:
  0.0 456.1 jit_solution(640396169059032821)
XLA Ops:
  6.5 0.0 all-gather.3.cloned.1.call-start
  6.5 0.7 all-gather.3.cloned.1.call-update
  7.3 0.0 all-gather.5.cloned.1.call-start
  7.3 0.7 all-gather.5.cloned.1.call-update
  8.0 0.0 reduce-scatter.4.cloned.1.call-start
  8.1 0.5 collective-permute-start
  8.6 9.0 %collective-permute-done = bf16[256,1024]{1,0:T(8,128)(2,1)S(1)} collective-permute-done((bf16[256,1024]{1,0:T(8,128)(2,1)}, bf16[256,1024]{1,0:T(8,128)(2,1)S(1)}, u32[]{:S(2)}, u32[]{:S(2)}) %collective-permute-start) | collective-permute-done | bytes 524320 | tf_op jit(solution)/shard_map/ppermute | solution.py:46
  17.6 0.0 collective-permute-start.1
  17.6 8.6 %collective-permute-done.1 = bf16[256,1024]{1,0:T(8,128)(2,1)S(1)} collective-permute-done((bf16[256,1024]{1,0:T(8,128)(2,1)S(1)}, bf16[256,1024]{1,0:T(8,128)(2,1)S(1)}, u32[]{:S(2)}, u32[]{:S(2)}) %collective-permute-start.1) | collective-permute-done | bytes 524320 | tf_op jit(solution)/shard_map/ppermute | solution.py:46
  26.2 0.0 collective-permute-start.2
  26.2 1.0 fusion.259
  27.2 0.8 fusion.260
  28.0 6.9 %collective-permute-done.2 = bf16[256,1024]{1,0:T(8,128)(2,1)} collective-permute-done((bf16[256,1024]{1,0:T(8,128)(2,1)S(1)}, bf16[256,1024]{1,0:T(8,128)(2,1)}, u32[]{:S(2)}, u32[]{:S(2)}) %collective-permute-start.2) | collective-permute-done | bytes 524320 | tf_op jit(solution)/shard_map/ppermute | solution.py:46
  34.9 4.2 fusion
  39.1 87.9 %all-gather.3.cloned.1.call-done = bf16[3,4096,256]{2,1,0:T(8,128)(2,1)} async-done(((bf16[3,1024,256]{2,1,0:T(8,128)(2,1)}), bf16[3,4096,256]{2,1,0:T(8,128)(2,1)}) %all-gather.3.cloned.1.call-update) | async-done | bytes 6291472 | tf_op jit(solution)/shard_map/all_gather | solution.py:35
  127.0 2.3 fusion.45
  129.3 1.3 collective-permute-start.3
  130.7 1.3 collective-permute-done.3
  132.0 110.1 %all-gather.5.cloned.1.call-done = bf16[3,256,4096]{2,1,0:T(8,128)(2,1)} async-done(((bf16[3,256,1024]{2,1,0:T(8,128)(2,1)}), bf16[3,256,4096]{2,1,0:T(8,128)(2,1)}) %all-gather.5.cloned.1.call-update) | async-done | bytes 6291472 | tf_op jit(solution)/shard_map/all_gather | solution.py:36
  242.1 0.0 copy-start.1
  242.1 4.4 convolution_convert_fusion.2
  246.5 0.0 reduce-scatter.4.cloned.1.call-update
  246.5 0.0 reduce-scatter.6.cloned.1.call-start
  246.6 0.0 copy-done.1
  246.7 29.4 %reduce-scatter.4.cloned.1.call-done = bf16[256,1024]{1,0:T(8,128)(2,1)} async-done(((bf16[256,4096]{1,0:T(8,128)(2,1)}), bf16[256,1024]{1,0:T(8,128)(2,1)}) %reduce-scatter.4.cloned.1.call-update) | async-done | bytes 524304 | tf_op jit(solution)/shard_map/reduce_scatter | solution.py:66
  276.1 1.2 fusion.54
  277.3 5.8 %psum.21 = f32[256]{0:T(256)S(1)} all-reduce(f32[256]{0:T(256)S(1)} %fusion.54), channel_id=1, replica_groups=mesh['grp'=2,'sp'=4,'tp'=4] {'tp'}, use_global_device_ids=true, to_apply=%region_3.5 | all-reduce | flops 256 | bytes 2048 | tf_op jit(solution)/shard_map/psum | solution.py:69
  283.0 0.0 copy-done
  283.1 1.3 fusion.57
  284.4 0.1 collective-permute-start.4
  284.4 8.6 %collective-permute-done.4 = bf16[256,1024]{1,0:T(8,128)(2,1)S(1)} collective-permute-done((bf16[256,1024]{1,0:T(8,128)(2,1)S(1)}, bf16[256,1024]{1,0:T(8,128)(2,1)S(1)}, u32[]{:S(2)}, u32[]{:S(2)}) %collective-permute-start.4) | collective-permute-done | bytes 524320 | tf_op jit(solution)/shard_map/ppermute | solution.py:46
  293.0 0.0 collective-permute-start.5
  293.0 8.6 %collective-permute-done.5 = bf16[256,1024]{1,0:T(8,128)(2,1)S(1)} collective-permute-done((bf16[256,1024]{1,0:T(8,128)(2,1)S(1)}, bf16[256,1024]{1,0:T(8,128)(2,1)S(1)}, u32[]{:S(2)}, u32[]{:S(2)}) %collective-permute-start.5) | collective-permute-done | bytes 524320 | tf_op jit(solution)/shard_map/ppermute | solution.py:46
  301.6 0.0 collective-permute-start.6
  301.6 8.6 %collective-permute-done.6 = bf16[256,1024]{1,0:T(8,128)(2,1)S(1)} collective-permute-done((bf16[256,1024]{1,0:T(8,128)(2,1)S(1)}, bf16[256,1024]{1,0:T(8,128)(2,1)S(1)}, u32[]{:S(2)}, u32[]{:S(2)}) %collective-permute-start.6) | collective-permute-done | bytes 524320 | tf_op jit(solution)/shard_map/ppermute | solution.py:46
  310.2 3.7 fusion.3
  313.9 0.0 copy-start.2
  314.0 2.4 fusion.48
  316.4 3.6 collective-permute-start.7
  320.0 1.3 collective-permute-done.7
  321.4 0.0 copy-done.2
  321.4 4.3 convolution_convert_fusion.1
  325.7 0.0 reduce-scatter.6.cloned.1.call-update
  325.7 0.0 reduce-scatter.8.cloned.1.call-start
  325.8 32.5 %reduce-scatter.6.cloned.1.call-done = bf16[256,1024]{1,0:T(8,128)(2,1)} async-done(((bf16[256,4096]{1,0:T(8,128)(2,1)}), bf16[256,1024]{1,0:T(8,128)(2,1)}) %reduce-scatter.6.cloned.1.call-update) | async-done | bytes 524304 | tf_op jit(solution)/shard_map/reduce_scatter | solution.py:66
  358.3 1.2 fusion.58
  359.5 5.8 %psum.22 = f32[256]{0:T(256)S(1)} all-reduce(f32[256]{0:T(256)S(1)} %fusion.58), channel_id=1, replica_groups=mesh['grp'=2,'sp'=4,'tp'=4] {'tp'}, use_global_device_ids=true, to_apply=%region_7.9 | all-reduce | flops 256 | bytes 2048 | tf_op jit(solution)/shard_map/psum | solution.py:69
  365.3 1.3 fusion.61
  366.6 0.1 collective-permute-start.8
  366.7 8.6 %collective-permute-done.8 = bf16[256,1024]{1,0:T(8,128)(2,1)S(1)} collective-permute-done((bf16[256,1024]{1,0:T(8,128)(2,1)S(1)}, bf16[256,1024]{1,0:T(8,128)(2,1)S(1)}, u32[]{:S(2)}, u32[]{:S(2)}) %collective-permute-start.8) | collective-permute-done | bytes 524320 | tf_op jit(solution)/shard_map/ppermute | solution.py:46
  375.3 0.0 collective-permute-start.9
  375.3 8.6 %collective-permute-done.9 = bf16[256,1024]{1,0:T(8,128)(2,1)S(1)} collective-permute-done((bf16[256,1024]{1,0:T(8,128)(2,1)S(1)}, bf16[256,1024]{1,0:T(8,128)(2,1)S(1)}, u32[]{:S(2)}, u32[]{:S(2)}) %collective-permute-start.9) | collective-permute-done | bytes 524320 | tf_op jit(solution)/shard_map/ppermute | solution.py:46
  383.9 0.0 collective-permute-start.10
  383.9 8.6 %collective-permute-done.10 = bf16[256,1024]{1,0:T(8,128)(2,1)S(1)} collective-permute-done((bf16[256,1024]{1,0:T(8,128)(2,1)S(1)}, bf16[256,1024]{1,0:T(8,128)(2,1)S(1)}, u32[]{:S(2)}, u32[]{:S(2)}) %collective-permute-start.10) | collective-permute-done | bytes 524320 | tf_op jit(solution)/shard_map/ppermute | solution.py:46
  392.5 3.7 fusion.6
  396.2 2.4 fusion.51
  398.6 3.6 collective-permute-start.11
  402.2 1.3 collective-permute-done.11
  403.6 4.3 convolution_convert_fusion
  407.9 0.0 reduce-scatter.8.cloned.1.call-update
  407.9 32.5 %reduce-scatter.8.cloned.1.call-done = bf16[256,1024]{1,0:T(8,128)(2,1)} async-done(((bf16[256,4096]{1,0:T(8,128)(2,1)}), bf16[256,1024]{1,0:T(8,128)(2,1)}) %reduce-scatter.8.cloned.1.call-update) | async-done | bytes 524304 | tf_op jit(solution)/shard_map/reduce_scatter | solution.py:66
  440.4 1.2 fusion.62
  441.7 5.8 %psum.23 = f32[256]{0:T(256)S(1)} all-reduce(f32[256]{0:T(256)S(1)} %fusion.62), channel_id=1, replica_groups=mesh['grp'=2,'sp'=4,'tp'=4] {'tp'}, use_global_device_ids=true, to_apply=%region_11.13 | all-reduce | flops 256 | bytes 2048 | tf_op jit(solution)/shard_map/psum | solution.py:69
  447.4 2.1 fusion.65
  (18 shorter events, 0.2 us)
Async XLA Ops:
  6.5 120.4 %all-gather.3.cloned.1.call-start = ((), (), s32[]{:S(2)}) async-start(), calls=%async_computation.3 | async-start | bytes 7864320 | tf_op jit(solution)/shard_map/all_gather | solution.py:35
  7.3 234.8 %all-gather.5.cloned.1.call-start = ((), (), s32[]{:S(2)}) async-start(), calls=%async_computation.4 | async-start | bytes 7864320 | tf_op jit(solution)/shard_map/all_gather | solution.py:36
  8.0 268.1 %reduce-scatter.4.cloned.1.call-start = ((), (), s32[]{:S(2)}) async-start(), calls=%async_computation.5 | async-start | bytes 2621440 | tf_op jit(solution)/shard_map/reduce_scatter | solution.py:66
  8.1 9.5 %collective-permute-start = (bf16[256,1024]{1,0:T(8,128)(2,1)}, bf16[256,1024]{1,0:T(8,128)(2,1)S(1)}, u32[]{:S(2)}, u32[]{:S(2)}) collective-permute-start(bf16[256,1024]{1,0:T(8,128)(2,1)} %param.9), channel_id=1, source_target_pairs={{0,1},{1,2},{2,3},{3,0},{4,5},{5,6},{6,7},{7,4},{8,9},{9,10},{10,1... | collective-permute-start | bytes 1572872 | tf_op jit(solution)/shard_map/ppermute | solution.py:46
  17.6 8.6 %collective-permute-start.1 = (bf16[256,1024]{1,0:T(8,128)(2,1)S(1)}, bf16[256,1024]{1,0:T(8,128)(2,1)S(1)}, u32[]{:S(2)}, u32[]{:S(2)}) collective-permute-start(bf16[256,1024]{1,0:T(8,128)(2,1)S(1)} %collective-permute-done), channel_id=1, source_target_pairs={{0,1},{1,2},{2,3},{3,0},{4,5},{5,6},{6,7},{7,4},{8,9},{9,10},{10,1... | collective-permute-start | bytes 1572872 | tf_op jit(solution)/shard_map/ppermute | solution.py:46
  26.2 8.7 %collective-permute-start.2 = (bf16[256,1024]{1,0:T(8,128)(2,1)S(1)}, bf16[256,1024]{1,0:T(8,128)(2,1)}, u32[]{:S(2)}, u32[]{:S(2)}) collective-permute-start(bf16[256,1024]{1,0:T(8,128)(2,1)S(1)} %collective-permute-done.1), channel_id=1, source_target_pairs={{0,1},{1,2},{2,3},{3,0},{4,5},{5,6},{6,7},{7,4},{8,9},{9,10},{10,1... | collective-permute-start | bytes 1572872 | tf_op jit(solution)/shard_map/ppermute | solution.py:46
  129.3 2.6 collective-permute-start.3
  242.1 4.5 copy-start.1
  242.1 41.0 %copy-start = (bf16[256,1024]{1,0:T(8,128)(2,1)S(1)}, bf16[256,1024]{1,0:T(8,128)(2,1)}, u32[]{:S(2)}) copy-start(bf16[256,1024]{1,0:T(8,128)(2,1)} %param.9) | copy-start | bytes 1572868
  246.5 111.8 %reduce-scatter.6.cloned.1.call-start = ((), (), s32[]{:S(2)}) async-start(), calls=%async_computation.6 | async-start | bytes 2621440 | tf_op jit(solution)/shard_map/reduce_scatter | solution.py:66
  284.4 8.7 %collective-permute-start.4 = (bf16[256,1024]{1,0:T(8,128)(2,1)S(1)}, bf16[256,1024]{1,0:T(8,128)(2,1)S(1)}, u32[]{:S(2)}, u32[]{:S(2)}) collective-permute-start(bf16[256,1024]{1,0:T(8,128)(2,1)S(1)} %fusion.57), channel_id=1, source_target_pairs={{0,1},{1,2},{2,3},{3,0},{4,5},{5,6},{6,7},{7,4},{8,9},{9,10},{10,1... | collective-permute-start | bytes 1572872 | tf_op jit(solution)/shard_map/ppermute | solution.py:46
  293.0 8.6 %collective-permute-start.5 = (bf16[256,1024]{1,0:T(8,128)(2,1)S(1)}, bf16[256,1024]{1,0:T(8,128)(2,1)S(1)}, u32[]{:S(2)}, u32[]{:S(2)}) collective-permute-start(bf16[256,1024]{1,0:T(8,128)(2,1)S(1)} %collective-permute-done.4), channel_id=1, source_target_pairs={{0,1},{1,2},{2,3},{3,0},{4,5},{5,6},{6,7},{7,4},{8,9},{9,10},{10,1... | collective-permute-start | bytes 1572872 | tf_op jit(solution)/shard_map/ppermute | solution.py:46
  301.6 8.6 %collective-permute-start.6 = (bf16[256,1024]{1,0:T(8,128)(2,1)S(1)}, bf16[256,1024]{1,0:T(8,128)(2,1)S(1)}, u32[]{:S(2)}, u32[]{:S(2)}) collective-permute-start(bf16[256,1024]{1,0:T(8,128)(2,1)S(1)} %collective-permute-done.5), channel_id=1, source_target_pairs={{0,1},{1,2},{2,3},{3,0},{4,5},{5,6},{6,7},{7,4},{8,9},{9,10},{10,1... | collective-permute-start | bytes 1572872 | tf_op jit(solution)/shard_map/ppermute | solution.py:46
  313.9 7.4 %copy-start.2 = (bf16[3,1,256,256]{3,2,1,0:T(8,128)(2,1)S(1)}, bf16[3,1,256,256]{3,2,1,0:T(8,128)(2,1)}, u32[]{:S(2)}) copy-start(bf16[3,1,256,256]{3,2,1,0:T(8,128)(2,1)} %param.12) | copy-start | bytes 1179652
  316.4 4.9 %collective-permute-start.7 = (bf16[15,256]{1,0:T(8,128)(2,1)S(1)}, bf16[15,256]{1,0:T(8,128)(2,1)S(1)}, u32[]{:S(2)}, u32[]{:S(2)}) collective-permute-start(bf16[15,256]{1,0:T(8,128)(2,1)S(1)} %slice.296), channel_id=1, source_target_pairs={{0,4},{4,8},{8,12},{1,5},{5,9},{9,13},{2,6},{6,10},{10,14},{3,7},{... | collective-permute-start | bytes 23048 | tf_op jit(solution)/shard_map/ppermute | solution.py:14
  325.7 114.7 %reduce-scatter.8.cloned.1.call-start = ((), (), s32[]{:S(2)}) async-start(), calls=%async_computation.7 | async-start | bytes 2621440 | tf_op jit(solution)/shard_map/reduce_scatter | solution.py:66
  366.6 8.7 %collective-permute-start.8 = (bf16[256,1024]{1,0:T(8,128)(2,1)S(1)}, bf16[256,1024]{1,0:T(8,128)(2,1)S(1)}, u32[]{:S(2)}, u32[]{:S(2)}) collective-permute-start(bf16[256,1024]{1,0:T(8,128)(2,1)S(1)} %fusion.61), channel_id=1, source_target_pairs={{0,1},{1,2},{2,3},{3,0},{4,5},{5,6},{6,7},{7,4},{8,9},{9,10},{10,1... | collective-permute-start | bytes 1572872 | tf_op jit(solution)/shard_map/ppermute | solution.py:46
  375.3 8.6 %collective-permute-start.9 = (bf16[256,1024]{1,0:T(8,128)(2,1)S(1)}, bf16[256,1024]{1,0:T(8,128)(2,1)S(1)}, u32[]{:S(2)}, u32[]{:S(2)}) collective-permute-start(bf16[256,1024]{1,0:T(8,128)(2,1)S(1)} %collective-permute-done.8), channel_id=1, source_target_pairs={{0,1},{1,2},{2,3},{3,0},{4,5},{5,6},{6,7},{7,4},{8,9},{9,10},{10,1... | collective-permute-start | bytes 1572872 | tf_op jit(solution)/shard_map/ppermute | solution.py:46
  383.9 8.6 %collective-permute-start.10 = (bf16[256,1024]{1,0:T(8,128)(2,1)S(1)}, bf16[256,1024]{1,0:T(8,128)(2,1)S(1)}, u32[]{:S(2)}, u32[]{:S(2)}) collective-permute-start(bf16[256,1024]{1,0:T(8,128)(2,1)S(1)} %collective-permute-done.9), channel_id=1, source_target_pairs={{0,1},{1,2},{2,3},{3,0},{4,5},{5,6},{6,7},{7,4},{8,9},{9,10},{10,1... | collective-permute-start | bytes 1572872 | tf_op jit(solution)/shard_map/ppermute | solution.py:46
  398.6 4.9 %collective-permute-start.11 = (bf16[15,256]{1,0:T(8,128)(2,1)S(1)}, bf16[15,256]{1,0:T(8,128)(2,1)S(1)}, u32[]{:S(2)}, u32[]{:S(2)}) collective-permute-start(bf16[15,256]{1,0:T(8,128)(2,1)S(1)} %slice.315), channel_id=1, source_target_pairs={{0,4},{4,8},{8,12},{1,5},{5,9},{9,13},{2,6},{6,10},{10,14},{3,7},{... | collective-permute-start | bytes 23048 | tf_op jit(solution)/shard_map/ppermute | solution.py:14
Sparse Core Ops, SparseCore 0:
  8.9 118.0 all-gather.2
  128.6 113.5 all-gather.4
  246.7 29.3 reduce-scatter.3
  325.8 32.4 reduce-scatter.5
  408.0 32.3 reduce-scatter.7
